TPU v7x, 32 devices: a whole 2x2x4 slice. The times are simulated.
32 devices in a mesh: sp: 8 (over z, y), tp: 4 (over x, core).
Axes of the slice: x: 2, y: 2, z: 4, core: 2. Of those that a mesh axis runs over, the one named last changes fastest.
Arguments:
- skip_stream: bfloat16 [2048, 2048], P('sp', 'tp'), may hold values from -20 to 20
- narrow_lookup_matrix: bfloat16 [2048, 256], P('sp', 'tp'), may hold values from -6 to 6
- narrow_probe_matrix: bfloat16 [2048, 256], P('sp', 'tp'), may hold values from -6 to 6
- narrow_retention_logits: bfloat16 [2048, 256], P('sp', 'tp'), may hold values from -6 to 16
- broad_lookup_matrix: bfloat16 [2048, 512], P('sp', 'tp'), may hold values from -6 to 6
- broad_probe_matrix: bfloat16 [2048, 512], P('sp', 'tp'), may hold values from -6 to 6
- broad_retention_logits: bfloat16 [2048, 512], P('sp', 'tp'), may hold values from -6 to 16
- content_vectors: bfloat16 [2048, 4, 2, 128], P('sp', 'tp'), may hold values from -6 to 6
- extra_log_retention: float32 [2048, 2, 4], P('sp', None, 'tp'), may hold values from -0.7 to 0
- per_branch_scaling: bfloat16 [4, 2, 128], P('tp'), may hold values from 0.099609375 to 1.8984375
- final_projection_matrix: bfloat16 [1024, 2048], P(None, 'tp'), may hold values from -0.1875 to 0.1875
- channel_blend_scaling: bfloat16 [2048], replicated, may hold values from 0.099609375 to 1.8984375
- switch_expansion_matrix: bfloat16 [2048, 5632], P('sp', 'tp'), may hold values from -0.125 to 0.125
- content_expansion_matrix: bfloat16 [2048, 5632], P('sp', 'tp'), may hold values from -0.125 to 0.125
- convolution_kernel: bfloat16 [3, 2, 5632], P(None, None, 'tp'), may hold values from -3.5 to 3.5
- contraction_matrix: bfloat16 [5632, 2048], P('tp', 'sp'), may hold values from -0.078125 to 0.078125
Outputs:
- mixed: bfloat16 [2048, 2048], P('sp', 'tp')
All inputs are finite; a program needn't handle non-finite values.
Results may differ from a plain program's by a relative error of at most 0.011.
Values may be sent and summed in bfloat16 or wider, within the bound.
A program may use at most 64 MiB of HBM per device.

v0:
```python
import jax
import jax.numpy as jnp
from jax import lax
from jax.sharding import PartitionSpec as P

BLOCK = 64
EPSILON = 1e-06
SOFTENING = 16.0
HIGHEST = lax.Precision.HIGHEST


def entering(value, axis, combine, identity):
    devices, mine = (lax.axis_size(axis), lax.axis_index(axis))
    everything = jax.tree.map(
        lambda part, kind: lax.all_gather(part.astype(kind), axis),
        value,
        jax.tree.map(lambda a: jnp.bfloat16 if a.dtype == jnp.float32 else a.dtype, value),
    )
    start = jax.tree.map(
        lambda part, zero: jnp.broadcast_to(jnp.asarray(zero, part.dtype), part.shape),
        value,
        identity,
    )

    def turn(k, before):
        reached = k < mine
        new = combine(
            before, jax.tree.map(lambda part, own: part[k].astype(own.dtype), everything, value)
        )
        return jax.tree.map(lambda a, b: jnp.where(reached, a, b), new, before)

    return lax.fori_loop(0, devices, turn, start)


def shifted(value, axis, steps):
    count = lax.axis_size(axis)
    initial, last = (max(0, -steps), min(count, count - steps))
    return lax.ppermute(value, axis, [(source, source + steps) for source in range(initial, last)])


def blocked(array):
    return array.reshape(array.shape[0] // BLOCK, BLOCK, array.shape[1], array.shape[2]).transpose(
        0, 2, 1, 3
    )


def group_parts(query_rows, input_keys, values_in, log_decay):
    query_blocks = blocked(query_rows)
    key_blocks = blocked(input_keys)
    value_blocks = blocked(values_in)
    inner = jnp.cumsum(blocked(log_decay), axis=2)
    last = inner[:, :, -1:, :]
    middle = inner[:, :, BLOCK // 2 - 1 : BLOCK // 2, :]
    scores = jnp.einsum(
        "nhid,nhjd->nhij",
        query_blocks * jnp.exp(inner - middle),
        key_blocks * jnp.exp(middle - inner),
        precision=HIGHEST,
    )
    lower = jnp.tril(jnp.ones((BLOCK, BLOCK), dtype=bool))
    local_out = jnp.einsum(
        "nhij,nhjv->nhiv", jnp.where(lower, scores, 0.0), value_blocks, precision=HIGHEST
    )
    query_carry = query_blocks * jnp.exp(inner)
    key_carry = key_blocks * jnp.exp(last - inner)
    block_logs = last[:, :, 0, :]
    fade = jnp.exp(block_logs)
    totals = jnp.sum(block_logs, axis=0)
    after = totals[None] - jnp.cumsum(block_logs, axis=0)
    summary = jnp.einsum(
        "nhjd,nhjv->hdv", key_carry * jnp.exp(after)[:, :, None, :], value_blocks, precision=HIGHEST
    )
    return ((local_out, query_carry, key_carry, value_blocks, fade), (jnp.exp(totals), summary))


def group_finish(parts, incoming):
    local_out, query_carry, key_carry, value_blocks, fade = parts

    def advance(state, inputs):
        query_part, key_part, value_part, fade_part = inputs
        output = jnp.einsum("hid,hdv->hiv", query_part, state, precision=HIGHEST)
        state = fade_part[..., None] * state + jnp.einsum(
            "hjd,hjv->hdv", key_part, value_part, precision=HIGHEST
        )
        return (state, output)

    _, carried = lax.scan(advance, incoming, (query_carry, key_carry, value_blocks, fade))
    total = local_out + carried
    return total.transpose(0, 2, 1, 3).reshape(-1, total.shape[1], total.shape[3])


def head_norm(output, gain):
    scale = lax.rsqrt(jnp.mean(output * output, axis=-1, keepdims=True) + EPSILON)
    return output * scale * gain.astype(jnp.float32)


def chain(earlier, later):
    joined = []
    for (fade_early, state_early), (fade_late, state_late) in zip(earlier, later):
        joined.append((fade_early * fade_late, fade_late[..., None] * state_early + state_late))
    return tuple(joined)


def convolve(upward, tap_rows):
    return tap_rows[0] * upward[:-2] + tap_rows[1] * upward[1:-1] + tap_rows[2] * upward[2:]


def local(
    skip_stream,
    narrow_lookup_matrix,
    narrow_probe_matrix,
    narrow_retention_logits,
    broad_lookup_matrix,
    broad_probe_matrix,
    broad_retention_logits,
    content_vectors,
    extra_log_retention,
    per_branch_scaling,
    final_projection_matrix,
    channel_blend_scaling,
    switch_expansion_matrix,
    content_expansion_matrix,
    convolution_kernel,
    contraction_matrix,
):
    item_count = skip_stream.shape[0]
    heads = content_vectors.shape[1]
    value_data = content_vectors.astype(jnp.float32)

    def build_arguments(query_rows, input_keys, forget_gates, spike_column):
        model_width = forget_gates.shape[1] // heads
        query_data = query_rows.astype(jnp.float32).reshape(
            item_count, heads, model_width
        ) * model_width ** (-0.5)
        key_data = input_keys.astype(jnp.float32).reshape(item_count, heads, model_width)
        decay_factor = (
            jax.nn.log_sigmoid(
                forget_gates.astype(jnp.float32).reshape(item_count, heads, model_width)
            )
            / SOFTENING
            + spike_column[:, :, None]
        )
        return (query_data, key_data, decay_factor)

    narrow_lookup_vector, narrow_probe_vector, narrow_probe_dim = build_arguments(
        narrow_lookup_matrix,
        narrow_probe_matrix,
        narrow_retention_logits,
        extra_log_retention[:, 0],
    )
    broad_lookup_vector, broad_probe_vector, broad_probe_dim = build_arguments(
        broad_lookup_matrix, broad_probe_matrix, broad_retention_logits, extra_log_retention[:, 1]
    )
    parts_small, summary_small = group_parts(
        narrow_lookup_vector, narrow_probe_vector, value_data[:, :, 0], narrow_probe_dim
    )
    parts_large, summary_large = group_parts(
        broad_lookup_vector, broad_probe_vector, value_data[:, :, 1], broad_probe_dim
    )
    identity = (
        (jnp.ones_like(summary_small[0]), jnp.zeros_like(summary_small[1])),
        (jnp.ones_like(summary_large[0]), jnp.zeros_like(summary_large[1])),
    )
    incoming = entering((summary_small, summary_large), "sp", chain, identity)
    out_small = group_finish(parts_small, incoming[0][1])
    out_large = group_finish(parts_large, incoming[1][1])
    stacked = jnp.stack(
        [
            head_norm(out_small, per_branch_scaling[:, 0]),
            head_norm(out_large, per_branch_scaling[:, 1]),
        ],
        axis=2,
    )
    heads_in = stacked.reshape(item_count, -1).astype(jnp.bfloat16)
    projected = jnp.dot(
        lax.all_gather(heads_in, "tp", axis=1, tiled=True),
        final_projection_matrix,
        preferred_element_type=jnp.float32,
    )
    resid_data = (
        (skip_stream.astype(jnp.float32) + projected).astype(jnp.bfloat16).astype(jnp.float32)
    )
    resid = resid_data.astype(jnp.bfloat16)
    whole = lax.all_gather(resid, "tp", axis=1, tiled=True).astype(jnp.float32)
    scale = lax.rsqrt(jnp.mean(whole * whole, axis=1, keepdims=True) + EPSILON)
    normed = (whole * scale * channel_blend_scaling.astype(jnp.float32)).astype(jnp.bfloat16)
    gate_rows, value_rows = (
        lax.all_gather(switch_expansion_matrix, "sp", axis=0, tiled=True),
        lax.all_gather(content_expansion_matrix, "sp", axis=0, tiled=True),
    )
    up_gate = jnp.dot(normed, gate_rows, preferred_element_type=jnp.float32).astype(jnp.bfloat16)
    up_value = jnp.dot(normed, value_rows, preferred_element_type=jnp.float32).astype(jnp.bfloat16)
    earlier_rows = shifted((up_value[-2:], up_gate[-2:]), "sp", 1)
    taps = convolution_kernel.astype(jnp.float32)
    value_ext = jnp.concatenate([earlier_rows[0], up_value], axis=0).astype(jnp.float32)
    gate_ext = jnp.concatenate([earlier_rows[1], up_gate], axis=0).astype(jnp.float32)
    conv_value = convolve(value_ext, taps[:, 0])
    conv_gate = convolve(gate_ext, taps[:, 1])
    hidden = (jax.nn.silu(conv_gate) * conv_value).astype(jnp.bfloat16)
    terms = jnp.dot(
        hidden,
        lax.all_gather(contraction_matrix, "sp", axis=1, tiled=True),
        preferred_element_type=jnp.float32,
    )
    down = lax.psum_scatter(
        terms.astype(jnp.bfloat16), "tp", scatter_dimension=1, tiled=True
    ).astype(jnp.float32)
    return (resid_data + down).astype(jnp.bfloat16)


def solution(mesh):
    in_specs = (
        P("sp", "tp"),
        P("sp", "tp"),
        P("sp", "tp"),
        P("sp", "tp"),
        P("sp", "tp"),
        P("sp", "tp"),
        P("sp", "tp"),
        P("sp", "tp", None, None),
        P("sp", None, "tp"),
        P("tp", None, None),
        P(None, "tp"),
        P(),
        P("sp", "tp"),
        P("sp", "tp"),
        P(None, None, "tp"),
        P("tp", "sp"),
    )
    out_specs = P("sp", "tp")
    return jax.shard_map(local, mesh=mesh, in_specs=in_specs, out_specs=out_specs, check_vma=False)
```

profile of v0, /device:TPU:0, one launch (start us, length us, event | category | flops | bytes accessed | tf_op | source)
XLA Modules:
  0.0 465.0 jit_solution(4777201416008957610)
XLA Ops:
  6.6 1.3 fusion.88
  7.9 1.2 fusion.87
  9.1 0.7 fusion.89
  9.8 1.0 fusion.56
  10.8 0.1 reduce_window_sum.51
  11.0 0.3 fusion.42
  11.3 32.6 %all-gather.3 = bf16[1024,128]{1,0:T(8,128)(2,1)S(1)} all-gather(bf16[128,128]{1,0:T(8,128)(2,1)S(1)} %fusion.42), channel_id=5, replica_groups=mesh['sp'=8,'tp'=4] {'sp'}, dimensions={0}, use_global_device_ids=true | all-gather | bytes 294912 | tf_op jit(solution)/shard_map/all_gather | solution.py:15
  44.1 0.1 reduce_window_sum.48
  44.3 0.1 copy.50
  44.4 0.3 fusion.43
  44.7 30.5 %all-gather.1 = bf16[512,128]{1,0:T(8,128)(2,1)S(1)} all-gather(bf16[64,128]{1,0:T(8,128)(2,1)S(1)} %fusion.43), channel_id=3, replica_groups=mesh['sp'=8,'tp'=4] {'sp'}, dimensions={0}, use_global_device_ids=true | all-gather | bytes 147456 | tf_op jit(solution)/shard_map/all_gather | solution.py:15
  75.2 0.6 dynamic-slice
  76.4 0.2 dynamic-update-slice
  76.6 21.4 %all-reduce = bf16[512]{0:T(512)(128)(2,1)S(1)} all-reduce(bf16[512]{0:T(512)(128)(2,1)S(1)} %dynamic-update-slice), channel_id=2, replica_groups=mesh['sp'=8,'tp'=4] {'sp'}, use_global_device_ids=true, to_apply=%add | all-reduce | flops 512 | bytes 2048
  98.1 16.3 %all-gather.4 = bf16[8,1,128]{2,1,0:T(2,128)(2,1)S(1)} all-gather(bf16[1,1,128]{2,1,0:T(2,128)(2,1)S(1)} %convert_bitcast_fusion), channel_id=4, replica_groups=mesh['sp'=8,'tp'=4] {'sp'}, dimensions={0}, use_global_device_ids=true | all-gather | bytes 2304 | tf_op jit(solution)/shard_map/all_gather | solution.py:15
  114.4 1.6 while.42
  114.6 0.1 fusion.136
  114.8 0.1 fusion.136
  116.2 1.8 while.40
  116.3 0.2 fusion.125
  116.4 0.2 fusion.124
  116.7 0.2 fusion.125
  116.9 0.2 fusion.124
  117.2 0.2 fusion.125
  117.4 0.2 fusion.124
  117.6 0.2 fusion.125
  117.8 0.2 fusion.124
  118.1 0.4 convolution_select_fusion.1
  118.4 0.3 multiply_reduce_fusion.1
  118.7 0.1 copy.62
  119.0 2.1 while.41
  119.1 0.2 fusion.132
  119.3 0.3 fusion.131
  119.6 0.2 fusion.132
  119.8 0.3 fusion.131
  120.1 0.2 fusion.132
  120.3 0.3 fusion.131
  120.7 0.2 fusion.132
  120.9 0.3 fusion.131
  121.2 0.4 convolution_select_fusion
  121.6 0.3 multiply_reduce_fusion
  121.9 0.1 copy.65
  122.1 0.1 multiply_convert_fusion
  122.2 7.2 %all_gather.41 = bf16[256,1024]{0,1:T(8,128)(2,1)S(1)} all-gather(bf16[256,256]{0,1:T(8,128)(2,1)S(1)} %bitcast.236), channel_id=1, replica_groups=mesh['sp'=8,'tp'=4] {'tp'}, dimensions={1}, use_global_device_ids=true | all-gather | bytes 655360 | tf_op jit(solution)/shard_map/all_gather | solution.py:176
  129.4 1.2 fusion.39
  130.6 0.7 all-gather.12.cloned.1.call-update
  131.4 0.7 all-gather.14.cloned.1.call-update
  132.1 0.5 all-gather.16.cloned.1.call-update
  132.9 12.6 %all-gather.10.cloned.1.call-done = bf16[256,2048]{1,0:T(8,128)(2,1)} async-done(((bf16[256,512]{1,0:T(8,128)(2,1)}), bf16[256,2048]{1,0:T(8,128)(2,1)}) %all-gather.10.cloned.1.call-update) | async-done | bytes 1048592 | tf_op jit(solution)/shard_map/all_gather | solution.py:184
  145.5 1.5 fusion.30
  147.0 93.0 %all-gather.12.cloned.1.call-done = bf16[2048,1408]{1,0:T(8,128)(2,1)} async-done(((bf16[256,1408]{1,0:T(8,128)(2,1)}), bf16[2048,1408]{1,0:T(8,128)(2,1)}) %all-gather.12.cloned.1.call-update) | async-done | bytes 5767184 | tf_op jit(solution)/shard_map/all_gather | solution.py:188
  240.0 4.8 %convolution_convert_fusion.1 = bf16[256,1408]{1,0:T(8,128)(2,1)S(1)} fusion(bf16[2048,1408]{1,0:T(8,128)(2,1)} %all-gather.12.cloned.1.call-done, bf16[256,2048]{1,0:T(8,128)(2,1)} %all-gather.10.cloned.1.call-done, f32[2048]{0:T(1024)S(1)} %convert_element_type.216, f32[256]{0:T(256)S(1)} %add_rsqrt_fusion.2), kind=kOutput, calls=%fused_computation.43 | convolution fusion | flops 1478852608 | bytes 7545856 | tf_op jit(solution)/shard_map/dot_general | solution.py:191
  244.8 0.9 copy-done.3
  245.7 2.5 collective-permute-start
  248.2 84.5 %all-gather.14.cloned.1.call-done = bf16[2048,1408]{1,0:T(8,128)(2,1)} async-done(((bf16[256,1408]{1,0:T(8,128)(2,1)}), bf16[2048,1408]{1,0:T(8,128)(2,1)}) %all-gather.14.cloned.1.call-update) | async-done | bytes 5767184 | tf_op jit(solution)/shard_map/all_gather | solution.py:189
  332.7 4.6 convolution_convert_fusion
  337.3 2.5 collective-permute-start.1
  339.8 0.2 maximum_convert_fusion
  339.9 1.1 collective-permute-done.1
  341.1 1.3 maximum_convert_fusion.1
  342.4 83.6 %all-gather.16.cloned.1.call-done = bf16[1408,2048]{1,0:T(8,128)(2,1)} async-done(((bf16[1408,256]{1,0:T(8,128)(2,1)}), bf16[1408,2048]{1,0:T(8,128)(2,1)}) %all-gather.16.cloned.1.call-update) | async-done | bytes 5767184 | tf_op jit(solution)/shard_map/all_gather | solution.py:202
  426.0 7.6 %convolution_convert_fusion.2 = bf16[256,2048]{1,0:T(8,128)(2,1)} fusion(bf16[1408,2048]{1,0:T(8,128)(2,1)} %all-gather.16.cloned.1.call-done, f32[258,1408]{1,0:T(8,128)} %maximum_convert_fusion.1, f32[258,1408]{1,0:T(8,128)S(1)} %maximum_convert_fusion, f32[1408]{0:T(1024)S(1)} %get-tuple-element.317, f32[1408]{0:T(1024)S(1)} %get-tuple-element.318, ...), kind=kOutput, calls=%fused_computation.44 | convolution fusion | flops 1482686464 | bytes 15515648 | tf_op jit(solution)/shard_map/dot_general | solution.py:200
  433.6 23.1 %reduce-scatter.2.cloned.1.call-done = bf16[256,512]{1,0:T(8,128)(2,1)} async-done(((bf16[256,2048]{1,0:T(8,128)(2,1)}), bf16[256,512]{1,0:T(8,128)(2,1)}) %reduce-scatter.2.cloned.1.call-update) | async-done | bytes 262160 | tf_op jit(solution)/shard_map/reduce_scatter | solution.py:205
  456.8 1.7 add_convert_fusion
  (112 shorter events, 2.7 us)
Async XLA Ops:
  6.5 122.9 %copy-start = (bf16[1024,512]{1,0:T(8,128)(2,1)S(1)}, bf16[1024,512]{1,0:T(8,128)(2,1)}, u32[]{:S(2)}) copy-start(bf16[1024,512]{1,0:T(8,128)(2,1)} %param.32) | copy-start | bytes 3145732
  6.5 4.5 copy-start.5
  6.5 37.4 %copy-start.7 = (bf16[256,64]{0,1:T(8,128)(2,1)S(1)}, bf16[256,64]{0,1:T(8,128)(2,1)}, u32[]{:S(2)}) copy-start(bf16[256,64]{0,1:T(8,128)(2,1)} %param.25) | copy-start | bytes 98308
  6.5 138.9 %all-gather.10.cloned.1.call-start = ((), (), s32[]{:S(2)}) async-start(), calls=%async_computation.1 | async-start | bytes 1310720 | tf_op jit(solution)/shard_map/all_gather | solution.py:184
  7.9 36.4 %copy-start.8 = (bf16[256,64]{0,1:T(8,128)(2,1)S(1)}, bf16[256,64]{0,1:T(8,128)(2,1)}, u32[]{:S(2)}) copy-start(bf16[256,64]{0,1:T(8,128)(2,1)} %param.24) | copy-start | bytes 98308
  9.8 65.4 %copy-start.14 = (u32[32]{0:T(128)S(1)}, u32[32]{0:T(128)}, u32[]{:S(2)}) copy-start(u32[32]{0:T(128)} %constant.109) | copy-start | bytes 388
  43.9 72.1 %copy-start.9 = (bf16[256,64]{0,1:T(8,128)(2,1)S(1)}, bf16[256,64]{0,1:T(8,128)(2,1)}, u32[]{:S(2)}) copy-start(bf16[256,64]{0,1:T(8,128)(2,1)} %param.23) | copy-start | bytes 98308
  116.2 2.7 copy-start.6
  119.0 3.1 copy-start.12
  121.2 8.2 %copy-start.13 = (bf16[256,512]{1,0:T(8,128)(2,1)S(1)}, bf16[256,512]{1,0:T(8,128)(2,1)}, u32[]{:S(2)}) copy-start(bf16[256,512]{1,0:T(8,128)(2,1)} %param.22) | copy-start | bytes 786436
  130.6 2.1 copy-start.11
  130.6 2.2 copy-start.10
  130.6 109.4 %all-gather.12.cloned.1.call-start = ((), (), s32[]{:S(2)}) async-start(), calls=%async_computation.2 | async-start | bytes 6488064 | tf_op jit(solution)/shard_map/all_gather | solution.py:188
  131.3 201.4 %all-gather.14.cloned.1.call-start = ((), (), s32[]{:S(2)}) async-start(), calls=%async_computation.3 | async-start | bytes 6488064 | tf_op jit(solution)/shard_map/all_gather | solution.py:189
  132.1 293.9 %all-gather.16.cloned.1.call-start = ((), (), s32[]{:S(2)}) async-start(), calls=%async_computation.4 | async-start | bytes 6488064 | tf_op jit(solution)/shard_map/all_gather | solution.py:202
  132.7 324.1 %reduce-scatter.2.cloned.1.call-start = ((), (), s32[]{:S(2)}) async-start(), calls=%async_computation.5 | async-start | bytes 1310720 | tf_op jit(solution)/shard_map/reduce_scatter | solution.py:205
  147.0 185.7 %copy-start.2 = (bf16[256,2048]{1,0:T(8,128)(2,1)S(1)}, bf16[256,2048]{1,0:T(8,128)(2,1)}, u32[]{:S(2)}) copy-start(bf16[256,2048]{1,0:T(8,128)(2,1)} %all-gather.10.cloned.1.call-done) | copy-start | bytes 3145732
  244.8 0.9 copy-start.3
  245.7 94.1 %collective-permute-start = (bf16[2,1408]{1,0:T(2,128)(2,1)S(1)}, bf16[2,1408]{1,0:T(2,128)(2,1)S(1)}, u32[]{:S(2)}, u32[]{:S(2)}) collective-permute-start(bf16[2,1408]{1,0:T(2,128)(2,1)S(1)} %slice.123), channel_id=1, source_target_pairs={{0,4},{4,8},{8,12},{12,16},{16,20},{20,24},{24,28},{1,5},{5,9},{9,... | collective-permute-start | bytes 16904 | tf_op jit(solution)/shard_map/ppermute | solution.py:38
  332.7 7.1 %copy-start.4 = (bf16[256,1408]{1,0:T(8,128)(2,1)S(1)}, bf16[256,1408]{1,0:T(8,128)(2,1)}, u32[]{:S(2)}) copy-start(bf16[256,1408]{1,0:T(8,128)(2,1)} %copy-done.3) | copy-start | bytes 2162692
  337.3 3.8 collective-permute-start.1
  426.0 30.8 %copy-start.1 = (bf16[256,512]{1,0:T(8,128)(2,1)S(1)}, bf16[256,512]{1,0:T(8,128)(2,1)}, u32[]{:S(2)}) copy-start(bf16[256,512]{1,0:T(8,128)(2,1)} %fusion.39) | copy-start | bytes 786436
Sparse Core Ops, SparseCore 0:
  130.7 14.7 all-gather.9
  147.7 92.3 all-gather.11
  242.2 90.4 all-gather.13
  334.6 91.3 all-gather.15
  433.8 22.9 reduce-scatter.1
where the time goes:
time: 465 us
  waiting for transfers between devices  300 us (65%)
  blocking collectives  108 us (23%)
  matrix products  23.7 us (5%)
  between operations  14.1 us (3%)
  other arithmetic  7.93 us (2%)
  local copies, waits for them, and re-layouts  5.9 us (1%)
  starting transfers between devices  5.07 us (1%)
    all_gather x1, waiting for transfers between devices, local(): lax.all_gather(switch_expansion_matrix, 'sp', axis=0, tiled=True)  93 us
    all_gather x1, waiting for transfers between devices, local(): lax.all_gather(content_expansion_matrix, 'sp', axis=0, tiled=True)  84.5 us
    all_gather x1, waiting for transfers between devices, local(): lax.all_gather(contraction_matrix, 'sp', axis=1, tiled=True)  83.6 us
    all_gather x3, blocking collectives, entering(): lax.all_gather(part.astype(kind), axis)  79.3 us
    reduce_scatter x1, waiting for transfers between devices, local(): lax.psum_scatter(terms.astype(jnp.bfloat16), 'tp', scatter_dimension=1, t...  23.1 us
    unnamed x1, blocking collectives  21.4 us
    all_gather x1, waiting for transfers between devices, local(): whole = lax.all_gather(resid, 'tp', axis=1, tiled=True).astype(jnp.float32)  12.6 us
  transfers between devices with their start and end apart: 7, of which 6 were waited for; matrix products, arithmetic and copies ran while one was open for 3% of the time, Pallas kernels for 0%

commit v1 on v0

--- a/solution.py
+++ b/solution.py
@@ -199,7 +199,7 @@
     hidden = (jax.nn.silu(conv_gate) * conv_value).astype(jnp.bfloat16)
     terms = jnp.dot(
         hidden,
-        lax.all_gather(contraction_matrix, "sp", axis=1, tiled=True),
+        jnp.concatenate(lax.all_gather(contraction_matrix, "sp"), axis=1),
         preferred_element_type=jnp.float32,
     )
     down = lax.psum_scatter(

time: 465 us -> 474 us (1.019)
  local copies, waits for them, and re-layouts: 5.9 us -> 15.1 us
    reshape x0 -> x1, local copies, waits for them, and re-layouts: none -> 8.3 us  [local(): jnp.concatenate(lax.all_gather(contraction_matrix, 'sp'), axis=1)]
  transfers between devices with their start and end apart: 7 -> 7, of which waited for: 6 -> 5; matrix products, arithmetic and copies ran while one was open for 3% -> 5% of each run, Pallas kernels for 0% -> 0%
where the time goes in v1:
time: 474 us; the launch traced here: 473 us
  waiting for transfers between devices  300 us (63%)
  blocking collectives  108 us (23%)
  matrix products  22.2 us (5%)
  local copies, waits for them, and re-layouts  15.1 us (3%)
  between operations  14.2 us (3%)
  other arithmetic  7.4 us (2%)
  starting transfers between devices  5.65 us (1%)
    all_gather x1, waiting for transfers between devices, local(): lax.all_gather(switch_expansion_matrix, 'sp', axis=0, tiled=True)  93 us
    all_gather x1, waiting for transfers between devices, local(): lax.all_gather(contraction_matrix, 'sp')  85.6 us
    all_gather x1, waiting for transfers between devices, local(): lax.all_gather(content_expansion_matrix, 'sp', axis=0, tiled=True)  84.2 us
    all_gather x3, blocking collectives, entering(): lax.all_gather(part.astype(kind), axis)  79.3 us
    reduce_scatter x1, waiting for transfers between devices, local(): lax.psum_scatter(terms.astype(jnp.bfloat16), 'tp', scatter_dimension=1, t...  23.1 us
    unnamed x1, blocking collectives  21.4 us
    all_gather x1, waiting for transfers between devices, local(): whole = lax.all_gather(resid, 'tp', axis=1, tiled=True).astype(jnp.float32)  12 us
  transfers between devices with their start and end apart: 7, of which 5 were waited for; matrix products, arithmetic and copies ran while one was open for 5% of the time, Pallas kernels for 0%

profile of v1, /device:TPU:0, one launch (start us, length us, event | category | flops | bytes accessed | tf_op | source)
XLA Modules:
  0.0 472.8 jit_solution(8109465501970935813)
XLA Ops:
  6.6 1.3 fusion.88
  7.9 1.2 fusion.87
  9.1 0.7 fusion.89
  9.8 0.8 fusion.79
  10.7 0.1 reduce_window_sum.48
  11.0 0.1 copy.69
  11.1 0.3 fusion.43
  11.4 32.3 %all-gather.1 = bf16[512,128]{1,0:T(8,128)(2,1)S(1)} all-gather(bf16[64,128]{1,0:T(8,128)(2,1)S(1)} %fusion.43), channel_id=3, replica_groups=mesh['sp'=8,'tp'=4] {'sp'}, dimensions={0}, use_global_device_ids=true | all-gather | bytes 147456 | tf_op jit(solution)/shard_map/all_gather | solution.py:15
  43.7 0.1 fusion.56
  43.8 0.1 reduce_window_sum.51
  44.1 0.3 fusion.42
  44.4 30.7 %all-gather.3 = bf16[1024,128]{1,0:T(8,128)(2,1)S(1)} all-gather(bf16[128,128]{1,0:T(8,128)(2,1)S(1)} %fusion.42), channel_id=5, replica_groups=mesh['sp'=8,'tp'=4] {'sp'}, dimensions={0}, use_global_device_ids=true | all-gather | bytes 294912 | tf_op jit(solution)/shard_map/all_gather | solution.py:15
  75.1 0.6 dynamic-slice
  76.4 0.2 dynamic-update-slice
  76.7 21.4 %all-reduce = bf16[512]{0:T(512)(128)(2,1)S(1)} all-reduce(bf16[512]{0:T(512)(128)(2,1)S(1)} %dynamic-update-slice), channel_id=2, replica_groups=mesh['sp'=8,'tp'=4] {'sp'}, use_global_device_ids=true, to_apply=%add | all-reduce | flops 512 | bytes 2048
  98.1 16.3 %all-gather.5 = bf16[8,1,128]{2,1,0:T(2,128)(2,1)S(1)} all-gather(bf16[1,1,128]{2,1,0:T(2,128)(2,1)S(1)} %convert_bitcast_fusion), channel_id=4, replica_groups=mesh['sp'=8,'tp'=4] {'sp'}, dimensions={0}, use_global_device_ids=true | all-gather | bytes 2304 | tf_op jit(solution)/shard_map/all_gather | solution.py:15
  114.4 1.6 while.42
  116.2 1.8 while.40
  116.2 0.2 fusion.125
  116.4 0.2 fusion.124
  116.7 0.2 fusion.125
  116.9 0.2 fusion.124
  117.2 0.2 fusion.125
  117.3 0.2 fusion.124
  117.6 0.2 fusion.125
  117.8 0.2 fusion.124
  118.1 0.4 convolution_select_fusion.1
  118.4 0.3 multiply_reduce_fusion.1
  118.7 0.1 copy.81
  119.0 2.1 while.41
  119.0 0.2 fusion.132
  119.3 0.3 fusion.131
  119.6 0.2 fusion.132
  119.8 0.3 fusion.131
  120.1 0.2 fusion.132
  120.3 0.3 fusion.131
  120.7 0.2 fusion.132
  120.9 0.3 fusion.131
  121.2 0.4 convolution_select_fusion
  121.6 0.3 multiply_reduce_fusion
  122.1 0.1 multiply_convert_fusion
  122.2 7.2 %all_gather.44 = bf16[256,1024]{0,1:T(8,128)(2,1)S(1)} all-gather(bf16[256,256]{0,1:T(8,128)(2,1)S(1)} %bitcast.242), channel_id=1, replica_groups=mesh['sp'=8,'tp'=4] {'tp'}, dimensions={1}, use_global_device_ids=true | all-gather | bytes 655360 | tf_op jit(solution)/shard_map/all_gather | solution.py:176
  129.4 1.2 fusion.39
  130.6 0.7 all-gather.13.cloned.1.call-update
  131.4 0.7 all-gather.15.cloned.1.call-update
  132.1 0.5 all-gather.17.cloned.1.call-update
  132.7 0.7 slice_reduce_fusion.5
  133.4 12.0 %all-gather.11.cloned.1.call-done = bf16[256,2048]{1,0:T(8,128)(2,1)} async-done(((bf16[256,512]{1,0:T(8,128)(2,1)}), bf16[256,2048]{1,0:T(8,128)(2,1)}) %all-gather.11.cloned.1.call-update) | async-done | bytes 1048592 | tf_op jit(solution)/shard_map/all_gather | solution.py:184
  145.5 1.5 fusion.30
  147.0 93.0 %all-gather.13.cloned.1.call-done = bf16[2048,1408]{1,0:T(8,128)(2,1)} async-done(((bf16[256,1408]{1,0:T(8,128)(2,1)}), bf16[2048,1408]{1,0:T(8,128)(2,1)}) %all-gather.13.cloned.1.call-update) | async-done | bytes 5767184 | tf_op jit(solution)/shard_map/all_gather | solution.py:188
  240.0 4.8 %convolution_convert_fusion.1 = bf16[256,1408]{1,0:T(8,128)(2,1)S(1)} fusion(bf16[2048,1408]{1,0:T(8,128)(2,1)} %all-gather.13.cloned.1.call-done, bf16[256,2048]{1,0:T(8,128)(2,1)} %all-gather.11.cloned.1.call-done, f32[2048]{0:T(1024)S(1)} %convert_element_type.216, f32[256]{0:T(256)S(1)} %add_rsqrt_fusion.2), kind=kOutput, calls=%fused_computation.43 | convolution fusion | flops 1478852608 | bytes 7545856 | tf_op jit(solution)/shard_map/dot_general | solution.py:191
  244.8 0.6 slice.123
  245.4 3.0 collective-permute-start
  248.5 84.2 %all-gather.15.cloned.1.call-done = bf16[2048,1408]{1,0:T(8,128)(2,1)} async-done(((bf16[256,1408]{1,0:T(8,128)(2,1)}), bf16[2048,1408]{1,0:T(8,128)(2,1)}) %all-gather.15.cloned.1.call-update) | async-done | bytes 5767184 | tf_op jit(solution)/shard_map/all_gather | solution.py:189
  332.7 4.5 convolution_convert_fusion
  337.2 2.5 collective-permute-start.1
  339.7 85.6 %all-gather.17.cloned.1.call-done = bf16[11264,256]{1,0:T(8,128)(2,1)} async-done(((bf16[1408,256]{1,0:T(8,128)(2,1)}), bf16[11264,256]{1,0:T(8,128)(2,1)}) %all-gather.17.cloned.1.call-update) | async-done | bytes 5767184 | tf_op jit(solution)/shard_map/all_gather | solution.py:202
  425.3 8.3 %copy.85 = bf16[1408,8,256]{0,2,1:T(8,128)(2,1)} copy(bf16[1408,8,256]{2,0,1:T(8,128)(2,1)} %bitcast.221) | data formatting | bytes 11534336 | tf_op jit(solution)/shard_map/reshape | solution.py:202
  433.6 0.8 maximum_convert_fusion
  434.5 0.2 maximum_convert_fusion.1
  434.6 0.5 copy-done.9
  435.2 6.3 %convolution_convert_fusion.2 = bf16[256,2048]{1,0:T(8,128)(2,1)} fusion(bf16[1408,2048]{0,1:T(8,128)(2,1)} %bitcast.222, f32[258,1408]{1,0:T(8,128)S(1)} %maximum_convert_fusion.1, f32[258,1408]{1,0:T(8,128)S(1)} %maximum_convert_fusion, f32[1408]{0:T(1024)S(1)} %copy-done.9, f32[1408]{0:T(1024)S(1)} %copy-done.10, f32[1408]{0:T(1024)S(1)} %copy-done.11, ...), kind=kOutput, calls=%fused_computation.44 | convolution fusion | flops 1482686464 | bytes 15515648 | tf_op jit(solution)/shard_map/dot_general | solution.py:200
  441.5 23.1 %reduce-scatter.2.cloned.1.call-done = bf16[256,512]{1,0:T(8,128)(2,1)} async-done(((bf16[256,2048]{1,0:T(8,128)(2,1)}), bf16[256,512]{1,0:T(8,128)(2,1)}) %reduce-scatter.2.cloned.1.call-update) | async-done | bytes 262160 | tf_op jit(solution)/shard_map/reduce_scatter | solution.py:205
  464.6 1.7 add_convert_fusion
  (121 shorter events, 2.9 us)
Async XLA Ops:
  6.5 122.8 %copy-start = (bf16[1024,512]{1,0:T(8,128)(2,1)S(1)}, bf16[1024,512]{1,0:T(8,128)(2,1)}, u32[]{:S(2)}) copy-start(bf16[1024,512]{1,0:T(8,128)(2,1)} %param.32) | copy-start | bytes 3145732
  6.5 4.4 copy-start.6
  6.5 37.2 %copy-start.3 = (bf16[256,128]{1,0:T(8,128)(2,1)S(1)}, bf16[256,128]{1,0:T(8,128)(2,1)}, u32[]{:S(2)}) copy-start(bf16[256,128]{1,0:T(8,128)(2,1)} %param.28) | copy-start | bytes 196612
  6.5 138.9 %all-gather.11.cloned.1.call-start = ((), (), s32[]{:S(2)}) async-start(), calls=%async_computation.1 | async-start | bytes 1310720 | tf_op jit(solution)/shard_map/all_gather | solution.py:184
  6.6 37.5 %copy-start.4 = (bf16[256,128]{1,0:T(8,128)(2,1)S(1)}, bf16[256,128]{1,0:T(8,128)(2,1)}, u32[]{:S(2)}) copy-start(bf16[256,128]{1,0:T(8,128)(2,1)} %param.27) | copy-start | bytes 196612
  9.8 65.3 %copy-start.18 = (u32[32]{0:T(128)S(1)}, u32[32]{0:T(128)}, u32[]{:S(2)}) copy-start(u32[32]{0:T(128)} %constant.109) | copy-start | bytes 388
  43.7 72.3 %copy-start.7 = (bf16[256,64]{0,1:T(8,128)(2,1)S(1)}, bf16[256,64]{0,1:T(8,128)(2,1)}, u32[]{:S(2)}) copy-start(bf16[256,64]{0,1:T(8,128)(2,1)} %param.23) | copy-start | bytes 98308
  116.2 2.7 copy-start.5
  119.0 3.0 copy-start.15
  121.2 8.2 %copy-start.17 = (bf16[256,512]{1,0:T(8,128)(2,1)S(1)}, bf16[256,512]{1,0:T(8,128)(2,1)}, u32[]{:S(2)}) copy-start(bf16[256,512]{1,0:T(8,128)(2,1)} %param.22) | copy-start | bytes 786436
  130.5 2.1 copy-start.14
  130.5 2.2 copy-start.8
  130.6 109.4 %all-gather.13.cloned.1.call-start = ((), (), s32[]{:S(2)}) async-start(), calls=%async_computation.2 | async-start | bytes 6488064 | tf_op jit(solution)/shard_map/all_gather | solution.py:188
  131.3 201.4 %all-gather.15.cloned.1.call-start = ((), (), s32[]{:S(2)}) async-start(), calls=%async_computation.3 | async-start | bytes 6488064 | tf_op jit(solution)/shard_map/all_gather | solution.py:189
  132.1 293.2 %all-gather.17.cloned.1.call-start = ((), (), s32[]{:S(2)}) async-start(), calls=%async_computation.5 | async-start | bytes 6488064 | tf_op jit(solution)/shard_map/all_gather | solution.py:202
  132.6 331.9 %reduce-scatter.2.cloned.1.call-start = ((), (), s32[]{:S(2)}) async-start(), calls=%async_computation.4 | async-start | bytes 1310720 | tf_op jit(solution)/shard_map/reduce_scatter | solution.py:205
  147.0 97.8 %copy-start.16 = (f32[256]{0:T(256)}, f32[256]{0:T(256)S(1)}, u32[]{:S(2)}) copy-start(f32[256]{0:T(256)S(1)} %add_rsqrt_fusion.2) | copy-start | bytes 3076
  147.0 185.7 %copy-start.2 = (bf16[256,2048]{1,0:T(8,128)(2,1)S(1)}, bf16[256,2048]{1,0:T(8,128)(2,1)}, u32[]{:S(2)}) copy-start(bf16[256,2048]{1,0:T(8,128)(2,1)} %all-gather.11.cloned.1.call-done) | copy-start | bytes 3145732
  245.4 188.1 %collective-permute-start = (bf16[2,1408]{1,0:T(2,128)(2,1)}, bf16[2,1408]{1,0:T(2,128)(2,1)}, u32[]{:S(2)}, u32[]{:S(2)}) collective-permute-start(bf16[2,1408]{1,0:T(2,128)(2,1)} %slice.123), channel_id=1, source_target_pairs={{0,4},{4,8},{8,12},{12,16},{16,20},{20,24},{24,28},{1,5},{5,9},{9,... | collective-permute-start | bytes 16904 | tf_op jit(solution)/shard_map/ppermute | solution.py:38
  337.2 97.2 %collective-permute-start.1 = (bf16[2,1408]{1,0:T(2,128)(2,1)S(1)}, bf16[2,1408]{1,0:T(2,128)(2,1)S(1)}, u32[]{:S(2)}, u32[]{:S(2)}) collective-permute-start(bf16[2,1408]{1,0:T(2,128)(2,1)S(1)} %slice.130), channel_id=1, source_target_pairs={{0,4},{4,8},{8,12},{12,16},{16,20},{20,24},{24,28},{1,5},{5,9},{9,... | collective-permute-start | bytes 16904 | tf_op jit(solution)/shard_map/ppermute | solution.py:38
  434.4 0.7 copy-start.9
  434.4 0.7 copy-start.10
  434.4 0.7 copy-start.11
  434.4 0.7 copy-start.12
  434.5 0.7 copy-start.13
  435.2 29.4 %copy-start.1 = (bf16[256,512]{1,0:T(8,128)(2,1)S(1)}, bf16[256,512]{1,0:T(8,128)(2,1)}, u32[]{:S(2)}) copy-start(bf16[256,512]{1,0:T(8,128)(2,1)} %fusion.39) | copy-start | bytes 786436
Sparse Core Ops, SparseCore 0:
  130.7 14.7 all-gather.10
  147.6 92.3 all-gather.12
  242.2 90.4 all-gather.14
  334.7 90.4 all-gather.16
  441.6 22.9 reduce-scatter.1
